TPU v7x, 512 devices: a whole 4x4x16 slice. The times are simulated.
512 devices in a mesh: rep: 2 (over z_hi), fs: 32 (over z_lo, y), tp: 8 (over x, core).
Axes of the slice: x: 4, y: 4, z: 16 (z_hi: 2, z_lo: 8; z = z_hi * 8 + z_lo), core: 2. Of those that a mesh axis runs over, the one named last changes fastest.
Arguments:
- tokens: bfloat16 [64, 1024, 1024], P(('rep', 'fs'), 'tp'), may hold values from -6 to 6
- mixer_in_gain: float32 [1024], replicated, may hold values from 0.5 to 1.5
- query_weight: bfloat16 [1024, 1024], P('fs', 'tp'), may hold values from -0.1875 to 0.1875
- key_weight: bfloat16 [1024, 1024], P('fs', 'tp'), may hold values from -0.1875 to 0.1875
- value_weight: bfloat16 [1024, 2048], P('fs', 'tp'), may hold values from -0.1875 to 0.1875
- gate_weight: bfloat16 [1024, 2048], P('fs', 'tp'), may hold values from -0.1875 to 0.1875
- decay_logits: float32 [2, 8], P(None, 'tp'), may hold values from 3.4 to 6.2
- mixer_output: bfloat16 [2048, 1024], P('tp', 'fs'), may hold values from -0.125 to 0.125
- mixer_out_gain: float32 [1024], replicated, may hold values from 0.5 to 1.5
- channel_in_gain: float32 [1024], replicated, may hold values from 0.5 to 1.5
- gelu_weight: bfloat16 [1024, 2816], P('fs', 'tp'), may hold values from -0.1875 to 0.1875
- linear_weight: bfloat16 [1024, 2816], P('fs', 'tp'), may hold values from -0.1875 to 0.1875
- gelu_kernel: float32 [3, 2816], P(None, 'tp'), may hold values from -3.5 to 3.5
- linear_kernel: float32 [3, 2816], P(None, 'tp'), may hold values from -3.5 to 3.5
- gelu_bias: float32 [2816], P('tp'), may hold values from -1.2 to 1.2
- linear_bias: float32 [2816], P('tp'), may hold values from -1.2 to 1.2
- down_weight: bfloat16 [2816, 1024], P('tp', 'fs'), may hold values from -0.109375 to 0.109375
- channel_out_gain: float32 [1024], replicated, may hold values from 0.5 to 1.5
Outputs:
- layer_output: bfloat16 [64, 1024, 1024], P(('rep', 'fs'), 'tp')
All inputs are finite; a program needn't handle non-finite values.
Results may differ from a plain program's by a relative error of at most 0.02.
Values may be sent and summed in bfloat16 or wider, within the bound.
No kernel may reach another device: no remote copies, remote signals or barrier semaphores. Data moves between devices by JAX's collectives and lax.ppermute only.
A program may use at most 64 MiB of HBM per device.

v0:
```python
import jax
import jax.numpy as jnp
from jax import lax
from jax.sharding import Mesh
from jax.sharding import PartitionSpec as P

DK = 128
DV = 256
SPAN = 128
TP = ("tp_0", "tp_1")
epsilon = 1e-06
rope_base = 10000.0


def joined_along(pieces, dim):
    lengths = list(pieces.shape[1:])
    lengths[dim] *= pieces.shape[0]
    return jnp.moveaxis(pieces, 0, dim).reshape(lengths)


def gather_together(arrays, axis, dims):
    flat = jnp.concatenate([a.reshape(-1) for a in arrays])
    lines, at, gathered = (lax.all_gather(flat, axis), 0, [])
    for a, dim in zip(arrays, dims):
        pieces = lines[:, at : at + a.size].reshape(-1, *a.shape)
        gathered.append(joined_along(pieces, dim))
        at += a.size
    return tuple(gathered)


def piece_ends(length, count):
    unit = 8 if length >= 8 * count else 1
    return [length // unit * k // count * unit for k in range(1, count)]


def all_blocks(value, axes, order):
    pieces = value[None]
    for k in order:
        pieces = lax.all_gather(pieces, axes[k], axis=0, tiled=True)
    carried = [lax.axis_size(axes[k]) for k in reversed(order)]
    pieces = pieces.reshape(*carried, *value.shape)
    turned = sorted(range(len(order)), key=lambda place: order[len(order) - 1 - place])
    return pieces.transpose(*turned, *range(len(order), pieces.ndim)).reshape(-1, *value.shape)


def gather_at_once(value, axes, dim):
    cut = max(range(max(1, value.ndim - 1)), key=lambda d: value.shape[d])
    count, gathered = (len(axes), [])
    for leading, piece in enumerate(
        jnp.split(value, piece_ends(value.shape[cut], count), axis=cut)
    ):
        if piece.size:
            order = [(leading - k) % count for k in range(count)]
            gathered.append(all_blocks(piece, axes, order))
    return joined_along(jnp.concatenate(gathered, axis=cut + 1), dim)


def on_whole(value, axes, dim, work):
    everything = gather_at_once(value, axes, dim)
    return work(everything, jnp.int32(0))


def own_rows_2(product, extent, axis):
    everything = product(jnp.int32(0), lax.axis_size(axis) * extent)
    own = lax.psum_scatter(everything.astype(jnp.bfloat16), axis, scatter_dimension=0, tiled=True)
    return own.astype(jnp.float32)


def rms_scaled(row_values, norm_gain):
    values = row_values.astype(jnp.float32)
    return (
        values * lax.rsqrt(jnp.mean(values * values, axis=-1, keepdims=True) + epsilon) * norm_gain
    )


def rotate(values, positions):
    half_width = values.shape[-1] // 2
    frequency = 1.0 / rope_base ** (jnp.arange(half_width, dtype=jnp.float32) / half_width)
    angles = positions.astype(jnp.float32)[:, None] * frequency[None, :]
    cosine = jnp.cos(angles)[:, None, :]
    sine_part = jnp.sin(angles)[:, None, :]
    first_half = values[..., :half_width]
    second = values[..., half_width:]
    return jnp.concatenate(
        [first_half * cosine - second * sine_part, first_half * sine_part + second * cosine],
        axis=-1,
    )


def one_direction(queries, key_rows, value_rows, log_decay, strict):
    highest = lax.Precision.HIGHEST
    length = queries.shape[0]
    head_count = queries.shape[1]
    block_count = length // SPAN
    inside_index = jnp.arange(SPAN, dtype=jnp.float32)
    offset = inside_index[:, None] - inside_index[None, :]
    allowed = offset >= (1.0 if strict else 0.0)
    within = jnp.where(
        allowed[None],
        jnp.exp(jnp.where(allowed, offset, 0.0)[None] * log_decay[:, None, None]),
        0.0,
    )
    query_blocks = queries.reshape(block_count, SPAN, head_count, -1)
    key_blocks = key_rows.reshape(block_count, SPAN, head_count, -1)
    value_blocks = value_rows.reshape(block_count, SPAN, head_count, -1).astype(jnp.float32)
    scores = (
        jnp.einsum("nchd,nmhd->nhcm", query_blocks, key_blocks, preferred_element_type=jnp.float32)
        * within[None]
    )
    inside = jnp.einsum("nhcm,nmhe->nche", scores, value_blocks, precision=highest)
    tail_decay = jnp.exp((SPAN - 1.0 - inside_index)[:, None] * log_decay[None, :])
    lead_decay = jnp.exp((inside_index + 1.0)[:, None] * log_decay[None, :])
    step_decay = jnp.exp(SPAN * log_decay)
    updates = jnp.einsum(
        "nmhd,nmhe->nhde",
        key_blocks.astype(jnp.float32),
        value_blocks * tail_decay[None, :, :, None],
        precision=highest,
    )

    def advance(carried, update):
        return (step_decay[:, None, None] * carried + update, carried)

    _, before = lax.scan(advance, jnp.zeros(updates.shape[1:], jnp.float32), updates)
    across = jnp.einsum(
        "nchd,nhde->nche",
        query_blocks.astype(jnp.float32) * lead_decay[None, :, :, None],
        before,
        precision=highest,
    )
    return (inside + across).reshape(length, head_count, -1)


def retention(queries, key_rows, value_rows, logits):
    log_forward = jax.nn.log_sigmoid(logits[0])
    log_backward = jax.nn.log_sigmoid(logits[1])
    forward = one_direction(queries, key_rows, value_rows, log_forward, False)
    behind = one_direction(queries[::-1], key_rows[::-1], value_rows[::-1], log_backward, True)[
        ::-1
    ]
    return forward + behind


def head_norm(values):
    centred = values - jnp.mean(values, axis=-1, keepdims=True)
    return centred * lax.rsqrt(jnp.mean(centred * centred, axis=-1, keepdims=True) + epsilon)


def conv_positions(values, kernel, biases):
    padded = jnp.pad(values.astype(jnp.float32), ((1, 1), (0, 0)))
    return kernel[0] * padded[:-2] + kernel[1] * padded[1:-1] + kernel[2] * padded[2:] + biases


def per_device(
    tokens,
    mixer_in_gain,
    query_weight,
    key_weight,
    value_weight,
    gate_weight,
    decay_logits,
    mixer_output,
    mixer_out_gain,
    channel_in_gain,
    gelu_weight,
    linear_weight,
    gelu_kernel,
    linear_kernel,
    gelu_bias,
    linear_bias,
    down_weight,
    channel_out_gain,
):
    token_rows = tokens[0]
    own_rows = token_rows.shape[0]
    normed = rms_scaled(token_rows, mixer_in_gain).astype(jnp.bfloat16)
    query_full, key_full, value_full, gate_full = gather_together(
        (query_weight, key_weight, value_weight, gate_weight), "fs", (0, 0, 0, 0)
    )
    query_width = query_full.shape[1]
    value_width = value_full.shape[1]
    head_count = query_width // DK

    def project(row_block, first_row):
        row_total = row_block.shape[0]
        positions = first_row + jnp.arange(row_total, dtype=jnp.int32)
        query_raw = jnp.dot(row_block, query_full, preferred_element_type=jnp.float32).reshape(
            row_total, head_count, DK
        )
        query_part = rotate(query_raw, positions).reshape(row_total, query_width)
        key_raw = jnp.dot(row_block, key_full, preferred_element_type=jnp.float32).reshape(
            row_total, head_count, DK
        )
        key_part = (rotate(key_raw, positions) * DK ** (-0.5)).reshape(row_total, query_width)
        value_part = jnp.dot(row_block, value_full, preferred_element_type=jnp.float32)
        gate_part = jnp.dot(row_block, gate_full, preferred_element_type=jnp.float32)
        return jnp.concatenate([query_part, key_part, value_part, gate_part], axis=1).astype(
            jnp.bfloat16
        )

    joined = on_whole(normed, TP, 0, project)
    length = joined.shape[0]
    queries = joined[:, :query_width].reshape(length, head_count, DK)
    key_rows = joined[:, query_width : 2 * query_width].reshape(length, head_count, DK)
    value_rows = joined[:, 2 * query_width : 2 * query_width + value_width].reshape(
        length, head_count, DV
    )
    gate_rows = joined[:, 2 * query_width + value_width :]
    retained = retention(queries, key_rows, value_rows, decay_logits)
    gated = (
        head_norm(retained).reshape(length, value_width)
        * jax.nn.silu(gate_rows.astype(jnp.float32))
    ).astype(jnp.bfloat16)
    output_columns = lax.all_gather(mixer_output, "fs", axis=1, tiled=True)

    def mixer_term(first_row, row_count):
        row_part = lax.dynamic_slice_in_dim(gated, first_row, row_count, 0)
        return jnp.dot(row_part, output_columns, preferred_element_type=jnp.float32)

    mix_sum = own_rows_2(mixer_term, own_rows, TP)
    after_mix = (token_rows.astype(jnp.float32) + rms_scaled(mix_sum, mixer_out_gain)).astype(
        jnp.bfloat16
    )
    channel_in = rms_scaled(after_mix, channel_in_gain).astype(jnp.bfloat16)
    gelu_full, linear_full = gather_together((gelu_weight, linear_weight), "fs", (0, 0))

    def expand(row_block, first_row):
        gelu_part = jnp.dot(row_block, gelu_full, preferred_element_type=jnp.float32)
        linear_part = jnp.dot(row_block, linear_full, preferred_element_type=jnp.float32)
        return jnp.concatenate([gelu_part, linear_part], axis=1).astype(jnp.bfloat16)

    both_parts = on_whole(channel_in, TP, 0, expand)
    gelu_in = both_parts[:, : gelu_full.shape[1]]
    linear_in = both_parts[:, gelu_full.shape[1] :]
    hidden = (
        jax.nn.gelu(conv_positions(gelu_in, gelu_kernel, gelu_bias))
        * conv_positions(linear_in, linear_kernel, linear_bias)
    ).astype(jnp.bfloat16)
    down_columns = lax.all_gather(down_weight, "fs", axis=1, tiled=True)

    def channel_term(first_row, row_count):
        row_part = lax.dynamic_slice_in_dim(hidden, first_row, row_count, 0)
        return jnp.dot(row_part, down_columns, preferred_element_type=jnp.float32)

    channel_sum = own_rows_2(channel_term, own_rows, TP)
    result = (after_mix.astype(jnp.float32) + rms_scaled(channel_sum, channel_out_gain)).astype(
        jnp.bfloat16
    )
    return result[None]


def solution(mesh):
    split = Mesh(
        mesh.devices.reshape(mesh.shape["rep"], mesh.shape["fs"], 4, 2),
        ("rep", "fs", "tp_0", "tp_1"),
    )
    in_specs = (
        P(("rep", "fs"), TP, None),
        P(),
        P("fs", TP),
        P("fs", TP),
        P("fs", TP),
        P("fs", TP),
        P(None, TP),
        P(TP, "fs"),
        P(),
        P(),
        P("fs", TP),
        P("fs", TP),
        P(None, TP),
        P(None, TP),
        P(TP),
        P(TP),
        P(TP, "fs"),
        P(),
    )
    out_specs = P(("rep", "fs"), TP, None)
    return jax.shard_map(
        per_device, mesh=split, in_specs=in_specs, out_specs=out_specs, check_vma=False
    )
```

profile of v0, /device:TPU:8, one launch (start us, length us, event | category | flops | bytes accessed | tf_op | source)
XLA Modules:
  0.0 770.2 jit_solution(12787065556506595714)
XLA Ops:
  6.5 1.1 fusion.44
  7.7 1.1 fusion.46
  8.8 13.9 %all-gather = bf16[256,1024]{1,0:T(8,128)(2,1)} all-gather(bf16[64,1024]{1,0:T(8,128)(2,1)S(1)} %get-tuple-element.171), channel_id=2, replica_groups=mesh['rep'=2,'fs'=32,'tp_0'=4,'tp_1'=2] {'tp_0'}, dimensions={0}, use_global_device_ids=true | all-gather | bytes 655360 | tf_op jit(solution)/shard_map/all_gather | solution.py:39
  22.8 2.1 all-gather.1
  28.7 124.4 %all_gather.48 = bf16[256,1024]{0,1:T(8,128)(2,1)} all-gather(bf16[256,32]{0,1:T(8,128)(2,1)S(1)} %copy-done.15), channel_id=1, replica_groups=mesh['rep'=2,'fs'=32,'tp_0'=4,'tp_1'=2] {'fs'}, dimensions={1}, use_global_device_ids=true | all-gather | bytes 540672 | tf_op jit(solution)/shard_map/all_gather | solution.py:214
  153.1 1.3 copy.35
  154.5 1.5 pad_maximum_fusion
  156.0 151.1 %all-gather.21.cloned.1.call-done = bf16[786432]{0:T(1024)(128)(2,1)} async-done(((bf16[24576]{0:T(1024)(128)(2,1)}), bf16[786432]{0:T(1024)(128)(2,1)}) %all-gather.21.cloned.1.call-update) | async-done | bytes 1572880 | tf_op jit(solution)/shard_map/all_gather | solution.py:23
  307.1 2.7 reshape.445
  309.8 1.1 fusion.98
  310.9 2.1 fusion.99
  313.9 1.8 convolution_bitcast_fusion.2
  316.5 1.9 fusion.71
  320.0 1.0 reshape_reshape.21
  321.0 1.7 convolution_convert_fusion.5
  323.4 1.8 fusion.48
  325.2 1.4 convolution_multiply_fusion.1
  326.6 1.5 fusion.104
  328.1 1.8 convolution_bitcast_fusion.1
  329.9 1.1 broadcast.305.clone.1
  331.0 13.0 %while.26 = (s32[]{:T(128)}, f32[1,128,256]{2,1,0:T(8,128)S(1)}, f32[8,1,128,256]{3,2,1,0:T(8,128)}, f32[1]{0:T(128)}, f32[8,1,128,256]{3,2,1,0:T(8,128)}, /*index=5*/s32[]{:T(128)}, s32[]{:T(128)}) while((s32[]{:T(128)}, f32[1,128,256]{2,1,0:T(8,128)S(1)}, f32[8,1,128,256]{3,2,1,0:T(8,128)}, f32[1]{0:T(128)}, ...), condition=%wide.region_2.3_spmd.clone, body=%wide.region_1.2_spmd.clone.sunk | while | flops 131075 | bytes 655968 | solution.py:124
  331.7 0.9 bitcast_add_fusion.6
  333.3 0.9 bitcast_add_fusion.6
  334.9 0.9 bitcast_add_fusion.6
  336.6 0.9 bitcast_add_fusion.6
  338.2 0.9 bitcast_add_fusion.6
  339.8 0.9 bitcast_add_fusion.6
  341.4 0.9 bitcast_add_fusion.6
  343.1 0.9 bitcast_add_fusion.6
  344.0 3.5 reverse.11
  347.6 2.9 reverse.10
  350.5 1.1 copy.48
  351.9 1.6 fusion.105
  353.4 1.8 convolution_bitcast_fusion
  355.2 1.1 broadcast.305.clone
  356.3 13.0 %while.27 = (s32[]{:T(128)}, f32[1,128,256]{2,1,0:T(8,128)S(1)}, f32[8,1,128,256]{3,2,1,0:T(8,128)}, f32[1]{0:T(128)}, f32[8,1,128,256]{3,2,1,0:T(8,128)}, /*index=5*/s32[]{:T(128)}, s32[]{:T(128)}) while((s32[]{:T(128)}, f32[1,128,256]{2,1,0:T(8,128)S(1)}, f32[8,1,128,256]{3,2,1,0:T(8,128)}, f32[1]{0:T(128)}, ...), condition=%wide.region_4.5_spmd.clone, body=%wide.region_3.4_spmd.clone.sunk | while | flops 131075 | bytes 655968 | solution.py:124
  357.0 0.9 bitcast_add_fusion.7
  358.6 0.9 bitcast_add_fusion.7
  365.1 0.9 bitcast_add_fusion.7
  369.3 3.3 convolution_add_fusion
  372.7 9.0 %rev.2 = f32[1024,1,256]{2,0,1:T(8,128)} reverse(f32[1024,1,256]{2,0,1:T(8,128)} %bitcast.150), dimensions={0} | reverse | bytes 2097152 | tf_op jit(solution)/shard_map/rev | solution.py:138
  381.6 2.4 convolution_add_fusion.1
  384.7 2.1 reshape_reshape.24
  386.8 4.7 convolution_convert_fusion.1
  393.2 38.3 %reduce-scatter.3.cloned.1.call-done = bf16[128,1024]{1,0:T(8,128)(2,1)} async-done(((bf16[1024,1024]{1,0:T(8,128)(2,1)}), bf16[128,1024]{1,0:T(8,128)(2,1)}) %reduce-scatter.3.cloned.1.call-update) | async-done | bytes 262160 | tf_op jit(solution)/shard_map/reduce_scatter | solution.py:65
  431.5 1.1 fusion.36
  432.6 1.2 fusion.40
  434.0 13.7 %all-gather.3 = bf16[256,1024]{1,0:T(8,128)(2,1)} all-gather(bf16[64,1024]{1,0:T(8,128)(2,1)S(1)} %get-tuple-element.167), channel_id=5, replica_groups=mesh['rep'=2,'fs'=32,'tp_0'=4,'tp_1'=2] {'tp_0'}, dimensions={0}, use_global_device_ids=true | all-gather | bytes 655360 | tf_op jit(solution)/shard_map/all_gather | solution.py:39
  447.8 122.5 %all_gather.55 = bf16[352,1024]{0,1:T(8,128)(2,1)} all-gather(bf16[352,32]{0,1:T(8,128)(2,1)S(1)} %copy-done.12), channel_id=1, replica_groups=mesh['rep'=2,'fs'=32,'tp_0'=4,'tp_1'=2] {'fs'}, dimensions={1}, use_global_device_ids=true | all-gather | bytes 743424 | tf_op jit(solution)/shard_map/all_gather | solution.py:239
  570.4 84.3 %all-gather.23.cloned.1.call-done = bf16[720896]{0:T(1024)(128)(2,1)} async-done(((bf16[22528]{0:T(1024)(128)(2,1)}), bf16[720896]{0:T(1024)(128)(2,1)}) %all-gather.23.cloned.1.call-update) | async-done | bytes 1441808 | tf_op jit(solution)/shard_map/all_gather | solution.py:23
  654.7 1.7 reshape.448
  656.5 2.1 all-gather.4
  658.8 2.1 reshape_reshape.26
  660.8 2.1 reshape_reshape.25
  662.9 11.5 %all-gather.17.cloned.1.call-done = bf16[8,64,1024]{2,1,0:T(8,128)(2,1)} async-done(((bf16[4,64,1024]{2,1,0:T(8,128)(2,1)}), bf16[8,64,1024]{2,1,0:T(8,128)(2,1)}) %all-gather.17.cloned.1.call-update) | async-done | bytes 1048592 | tf_op jit(solution)/shard_map/all_gather | solution.py:39
  674.4 1.3 copy.46
  675.8 33.9 %all-gather.19.cloned.1.call-done = bf16[8,64,1024]{2,1,0:T(8,128)(2,1)} async-done(((bf16[2,64,1024]{2,1,0:T(8,128)(2,1)}), bf16[8,64,1024]{2,1,0:T(8,128)(2,1)}) %all-gather.19.cloned.1.call-update) | async-done | bytes 1048592 | tf_op jit(solution)/shard_map/all_gather | solution.py:39
  709.6 1.5 pad_maximum_fusion.1
  711.2 1.0 fusion.19
  712.3 1.0 fusion.20
  713.5 4.8 convolution_convert_fusion
  718.3 42.1 %reduce-scatter.5.cloned.1.call-done = bf16[128,1024]{1,0:T(8,128)(2,1)} async-done(((bf16[1024,1024]{1,0:T(8,128)(2,1)}), bf16[128,1024]{1,0:T(8,128)(2,1)}) %reduce-scatter.5.cloned.1.call-update) | async-done | bytes 262160 | tf_op jit(solution)/shard_map/reduce_scatter | solution.py:65
  760.4 1.1 fusion.38
  761.5 1.8 fusion.74
  (130 shorter events, 24.9 us)
Async XLA Ops:
  6.5 146.6 %all-gather.13.cloned.1.call-start = ((), (), s32[]{:S(2)}) async-start(), calls=%async_computation.2 | async-start | bytes 1572864 | tf_op jit(solution)/shard_map/all_gather | solution.py:39
  7.6 17.4 %copy-start.16 = (bf16[32,256]{1,0:T(8,128)(2,1)S(1)}, bf16[32,256]{1,0:T(8,128)(2,1)}, u32[]{:S(2)}) copy-start(bf16[32,256]{1,0:T(8,128)(2,1)} %param.26) | copy-start | bytes 49156
  7.6 17.4 %copy-start.17 = (bf16[32,256]{1,0:T(8,128)(2,1)S(1)}, bf16[32,256]{1,0:T(8,128)(2,1)}, u32[]{:S(2)}) copy-start(bf16[32,256]{1,0:T(8,128)(2,1)} %param.27) | copy-start | bytes 49156
  7.7 17.4 %copy-start.18 = (bf16[32,128]{1,0:T(8,128)(2,1)S(1)}, bf16[32,128]{1,0:T(8,128)(2,1)}, u32[]{:S(2)}) copy-start(bf16[32,128]{1,0:T(8,128)(2,1)} %param.25) | copy-start | bytes 24580
  7.7 17.4 %copy-start.19 = (bf16[32,128]{1,0:T(8,128)(2,1)S(1)}, bf16[32,128]{1,0:T(8,128)(2,1)}, u32[]{:S(2)}) copy-start(bf16[32,128]{1,0:T(8,128)(2,1)} %param.24) | copy-start | bytes 24580
  7.7 18.1 %copy-start.25 = (f32[2,1]{0,1:T(1,128)S(1)}, f32[2,1]{0,1:T(1,128)}, u32[]{:S(2)}) copy-start(f32[2,1]{0,1:T(1,128)} %param.28) | copy-start | bytes 28
  8.8 19.9 %copy-start.15 = (bf16[256,32]{0,1:T(8,128)(2,1)S(1)}, bf16[256,32]{0,1:T(8,128)(2,1)}, u32[]{:S(2)}) copy-start(bf16[256,32]{0,1:T(8,128)(2,1)} %param.29) | copy-start | bytes 49156
  22.7 131.7 %all-gather.15.cloned.1.call-start = ((), (), s32[]{:S(2)}) async-start(), calls=%async_computation.3 | async-start | bytes 1310720 | tf_op jit(solution)/shard_map/all_gather | solution.py:39
  24.9 282.1 %all-gather.21.cloned.1.call-start = ((), (), s32[]{:S(2)}) async-start(), calls=%async_computation.8 | async-start | bytes 1622016 | tf_op jit(solution)/shard_map/all_gather | solution.py:23
  25.7 405.7 %reduce-scatter.3.cloned.1.call-start = ((), (), s32[]{:S(2)}) async-start(), calls=%async_computation.4 | async-start | bytes 2359296 | tf_op jit(solution)/shard_map/reduce_scatter | solution.py:65
  325.2 2.9 copy-start.3
  325.2 2.9 copy-start.4
  331.0 16.6 %copy-start.7 = (bf16[1024,128]{0,1:T(8,128)(2,1)S(1)}, bf16[1024,128]{0,1:T(8,128)(2,1)}, u32[]{:S(2)}) copy-start(bf16[1024,128]{0,1:T(8,128)(2,1)} %get-tuple-element.170) | copy-start | bytes 786436
  344.0 7.6 copy-start.11
  355.2 14.1 %copy-start.1 = (f32[8,256,128]{1,2,0:T(8,128)S(1)}, f32[8,256,128]{1,2,0:T(8,128)}, u32[]{:S(2)}) copy-start(f32[8,256,128]{1,2,0:T(8,128)} %fusion.105) | copy-start | bytes 3145732
  372.7 9.0 %copy-start = (f32[8,256,128]{1,2,0:T(8,128)S(1)}, f32[8,256,128]{1,2,0:T(8,128)}, u32[]{:S(2)}) copy-start(f32[8,256,128]{1,2,0:T(8,128)} %fusion.104) | copy-start | bytes 3145732
  372.7 9.0 %copy-start.6 = (bf16[1024,1,128]{2,0,1:T(8,128)(2,1)S(1)}, bf16[1024,1,128]{2,0,1:T(8,128)(2,1)}, u32[]{:S(2)}) copy-start(bf16[1024,1,128]{2,0,1:T(8,128)(2,1)} %copy.47) | copy-start | bytes 786436
  381.6 2.5 copy-start.2
  391.5 0.7 copy-start.13
  391.5 0.8 copy-start.14
  391.5 41.0 %copy-start.5 = (bf16[1,128,1024]{2,1,0:T(8,128)(2,1)S(1)}, bf16[1,128,1024]{2,1,0:T(8,128)(2,1)}, u32[]{:S(2)}) copy-start(bf16[1,128,1024]{2,1,0:T(8,128)(2,1)} %param.22) | copy-start | bytes 786436
  391.5 41.0 %copy-start.20 = (f32[1024]{0:T(1024)S(1)}, f32[1024]{0:T(1024)}, u32[]{:S(2)}) copy-start(f32[1024]{0:T(1024)} %param.30) | copy-start | bytes 12292
  391.5 42.3 %copy-start.21 = (f32[1024]{0:T(1024)S(1)}, f32[1024]{0:T(1024)}, u32[]{:S(2)}) copy-start(f32[1024]{0:T(1024)} %param.31) | copy-start | bytes 12292
  391.6 263.1 %all-gather.23.cloned.1.call-start = ((), (), s32[]{:S(2)}) async-start(), calls=%async_computation.9 | async-start | bytes 1486848 | tf_op jit(solution)/shard_map/all_gather | solution.py:23
  393.1 281.3 %all-gather.17.cloned.1.call-start = ((), (), s32[]{:S(2)}) async-start(), calls=%async_computation.5 | async-start | bytes 1572864 | tf_op jit(solution)/shard_map/all_gather | solution.py:39
  432.6 15.2 %copy-start.23 = (f32[3,352]{1,0:T(4,128)S(1)}, f32[3,352]{1,0:T(4,128)}, u32[]{:S(2)}) copy-start(f32[3,352]{1,0:T(4,128)} %param.35) | copy-start | bytes 12676
  432.6 15.2 %copy-start.24 = (f32[3,352]{1,0:T(4,128)S(1)}, f32[3,352]{1,0:T(4,128)}, u32[]{:S(2)}) copy-start(f32[3,352]{1,0:T(4,128)} %param.34) | copy-start | bytes 12676
  432.6 15.2 %copy-start.12 = (bf16[352,32]{0,1:T(8,128)(2,1)S(1)}, bf16[352,32]{0,1:T(8,128)(2,1)}, u32[]{:S(2)}) copy-start(bf16[352,32]{0,1:T(8,128)(2,1)} %param.38) | copy-start | bytes 67588
  447.7 261.9 %all-gather.19.cloned.1.call-start = ((), (), s32[]{:S(2)}) async-start(), calls=%async_computation.6 | async-start | bytes 1310720 | tf_op jit(solution)/shard_map/all_gather | solution.py:39
  658.6 101.8 %reduce-scatter.5.cloned.1.call-start = ((), (), s32[]{:S(2)}) async-start(), calls=%async_computation.7 | async-start | bytes 2359296 | tf_op jit(solution)/shard_map/reduce_scatter | solution.py:65
  709.6 1.5 copy-start.9
  711.2 1.1 copy-start.10
  712.3 1.1 copy-start.8
  712.3 1.1 copy-start.26
  712.3 1.1 copy-start.27
  718.3 43.3 %copy-start.22 = (f32[1024]{0:T(1024)S(1)}, f32[1024]{0:T(1024)}, u32[]{:S(2)}) copy-start(f32[1024]{0:T(1024)} %param.39) | copy-start | bytes 12292
Sparse Core Ops, SparseCore 0:
  22.9 23.9 all-gather.12
  48.9 33.0 all-gather.14
  84.1 222.8 all-gather.20
  391.7 39.7 reduce-scatter.2
  433.4 221.2 all-gather.22
  656.7 17.7 all-gather.16
  676.5 33.0 all-gather.18
  718.4 41.9 reduce-scatter.4
where the time goes:
time: 772 us; the launch traced here: 770 us
  waiting for transfers between devices  361 us (47%)
  blocking collectives  279 us (36%)
  other arithmetic  43.4 us (6%)
  local copies, waits for them, and re-layouts  40.7 us (5%)
  matrix products  29.9 us (4%)
  between operations  15.5 us (2%)
    all_gather x2, waiting for transfers between devices, gather_together(): lines, at, gathered = (lax.all_gather(flat, axis), 0, [])  235 us
    all_gather x1, blocking collectives, per_device(): output_columns = lax.all_gather(mixer_output, 'fs', axis=1, tiled=True)  124 us
    all_gather x1, blocking collectives, per_device(): down_columns = lax.all_gather(down_weight, 'fs', axis=1, tiled=True)  123 us
    reduce_scatter x2, waiting for transfers between devices, own_rows_2(): lax.psum_scatter(everything.astype(jnp.bfloat16), axis, scatter_dimension...  80.4 us
    all_gather x4, waiting for transfers between devices, all_blocks(): pieces = lax.all_gather(pieces, axes[k], axis=0, tiled=True)  45.4 us
    all_gather x4, blocking collectives, all_blocks(): pieces = lax.all_gather(pieces, axes[k], axis=0, tiled=True)  31.8 us
  transfers between devices with their start and end apart: 8, of which 6 were waited for; matrix products, arithmetic and copies ran while one was open for 2% of the time, Pallas kernels for 0%

commit v1 on v0

--- a/solution.py
+++ b/solution.py
@@ -36,7 +36,9 @@
 def all_blocks(value, axes, order):
     pieces = value[None]
     for k in order:
-        pieces = lax.all_gather(pieces, axes[k], axis=0, tiled=True)
+        pieces = jnp.concatenate(
+            lax.all_to_all(jnp.stack([pieces] * lax.axis_size(axes[k])), axes[k], 0, 0), axis=0
+        )
     carried = [lax.axis_size(axes[k]) for k in reversed(order)]
     pieces = pieces.reshape(*carried, *value.shape)
     turned = sorted(range(len(order)), key=lambda place: order[len(order) - 1 - place])

time: 772 us -> 677 us (0.88)
  the two profiles are of different devices: /device:TPU:8 before, /device:TPU:16 now
where the time goes in v1:
time: 677 us; the launch traced here: 675 us
  waiting for transfers between devices  257 us (38%)
  blocking collectives  254 us (38%)
  local copies, waits for them, and re-layouts  49.9 us (7%)
  other arithmetic  44.9 us (7%)
  matrix products  29.8 us (4%)
  starting transfers between devices  23.4 us (3%)
  between operations  15.2 us (2%)
    all_gather x2, waiting for transfers between devices, gather_together(): lines, at, gathered = (lax.all_gather(flat, axis), 0, [])  144 us
    all_gather x1, blocking collectives, per_device(): output_columns = lax.all_gather(mixer_output, 'fs', axis=1, tiled=True)  123 us
    all_gather x1, blocking collectives, per_device(): down_columns = lax.all_gather(down_weight, 'fs', axis=1, tiled=True)  122 us
    reduce_scatter x2, waiting for transfers between devices, own_rows_2(): lax.psum_scatter(everything.astype(jnp.bfloat16), axis, scatter_dimension...  94.2 us
    all_to_all x6, starting transfers between devices, all_blocks(): lax.all_to_all(jnp.stack([pieces] * lax.axis_size(axes[k])), axes[k], 0, 0)  23.3 us
    all_to_all x6, waiting for transfers between devices, all_blocks(): lax.all_to_all(jnp.stack([pieces] * lax.axis_size(axes[k])), axes[k], 0, 0)  18.5 us
    add x16, other arithmetic, advance(): return (step_decay[:, None, None] * carried + update, carried)  15.1 us
  transfers between devices with their start and end apart: 10, of which 8 were waited for; matrix products, arithmetic and copies ran while one was open for 3% of the time, Pallas kernels for 0%

profile of v1, /device:TPU:16, one launch (start us, length us, event | category | flops | bytes accessed | tf_op | source)
XLA Modules:
  0.0 674.7 jit_solution(8814025345174910351)
XLA Ops:
  8.0 1.3 pad_maximum_fusion.7
  9.4 1.1 fusion.44
  10.5 1.1 fusion.46
  12.4 4.3 all-to-all-start
  19.6 6.6 all-to-all-done
  26.2 3.4 all-to-all-start.2
  29.7 1.4 all-to-all-done.2
  31.2 4.6 all_to_all.40
  35.8 1.1 stack.27
  36.9 3.6 all-to-all-start.3
  41.8 123.3 %all_gather.20 = bf16[256,1024]{0,1:T(8,128)(2,1)} all-gather(bf16[256,32]{0,1:T(8,128)(2,1)S(1)} %copy-done.18), channel_id=1, replica_groups=mesh['rep'=2,'fs'=32,'tp_0'=4,'tp_1'=2] {'fs'}, dimensions={1}, use_global_device_ids=true | all-gather | bytes 540672 | tf_op jit(solution)/shard_map/all_gather | solution.py:216
  165.1 1.1 copy.31
  166.2 1.5 pad_maximum_fusion
  167.7 59.6 %all-gather.5.cloned.1.call-done = bf16[786432]{0:T(1024)(128)(2,1)} async-done(((bf16[24576]{0:T(1024)(128)(2,1)}), bf16[786432]{0:T(1024)(128)(2,1)}) %all-gather.5.cloned.1.call-update) | async-done | bytes 1572880 | tf_op jit(solution)/shard_map/all_gather | solution.py:23
  227.4 2.7 reshape.443
  230.1 1.1 fusion.98
  231.1 2.1 fusion.99
  234.2 1.8 convolution_bitcast_fusion.2
  236.8 1.9 fusion.71
  240.3 1.1 reshape_reshape.21
  241.4 1.7 convolution_convert_fusion.5
  243.8 1.8 fusion.48
  245.5 1.4 convolution_multiply_fusion.1
  246.9 1.6 fusion.104
  248.5 1.8 convolution_bitcast_fusion.1
  250.3 1.1 broadcast.311.clone.1
  251.4 13.0 %while.26 = (s32[]{:T(128)}, f32[1,128,256]{2,1,0:T(8,128)S(1)}, f32[8,1,128,256]{3,2,1,0:T(8,128)}, f32[1]{0:T(128)}, f32[8,1,128,256]{3,2,1,0:T(8,128)}, /*index=5*/s32[]{:T(128)}, s32[]{:T(128)}) while((s32[]{:T(128)}, f32[1,128,256]{2,1,0:T(8,128)S(1)}, f32[8,1,128,256]{3,2,1,0:T(8,128)}, f32[1]{0:T(128)}, ...), condition=%wide.region_2.3_spmd.clone, body=%wide.region_1.2_spmd.clone.sunk | while | flops 131075 | bytes 655968 | solution.py:126
  252.1 0.9 bitcast_add_fusion.6
  255.3 0.9 bitcast_add_fusion.6
  264.4 3.5 reverse.11
  268.0 2.9 reverse.10
  270.9 1.1 copy.44
  272.3 1.5 fusion.105
  273.8 1.8 convolution_bitcast_fusion
  275.6 1.1 broadcast.311.clone
  276.6 13.0 %while.27 = (s32[]{:T(128)}, f32[1,128,256]{2,1,0:T(8,128)S(1)}, f32[8,1,128,256]{3,2,1,0:T(8,128)}, f32[1]{0:T(128)}, f32[8,1,128,256]{3,2,1,0:T(8,128)}, /*index=5*/s32[]{:T(128)}, s32[]{:T(128)}) while((s32[]{:T(128)}, f32[1,128,256]{2,1,0:T(8,128)S(1)}, f32[8,1,128,256]{3,2,1,0:T(8,128)}, f32[1]{0:T(128)}, ...), condition=%wide.region_4.5_spmd.clone, body=%wide.region_3.4_spmd.clone.sunk | while | flops 131075 | bytes 655968 | solution.py:126
  278.9 0.9 bitcast_add_fusion.7
  289.7 3.4 convolution_add_fusion
  293.0 9.0 %rev.2 = f32[1024,1,256]{2,0,1:T(8,128)} reverse(f32[1024,1,256]{2,0,1:T(8,128)} %bitcast.154), dimensions={0} | reverse | bytes 2097152 | tf_op jit(solution)/shard_map/rev | solution.py:140
  302.0 2.4 convolution_add_fusion.1
  305.1 2.1 reshape_reshape.24
  307.2 4.7 convolution_convert_fusion.1
  314.2 46.9 %reduce-scatter.3.cloned.1.call-done = bf16[128,1024]{1,0:T(8,128)(2,1)} async-done(((bf16[1024,1024]{1,0:T(8,128)(2,1)}), bf16[128,1024]{1,0:T(8,128)(2,1)}) %reduce-scatter.3.cloned.1.call-update) | async-done | bytes 262160 | tf_op jit(solution)/shard_map/reduce_scatter | solution.py:67
  361.0 1.1 fusion.36
  362.1 1.2 fusion.40
  365.1 3.5 all-to-all-start.4
  368.6 121.7 %all_gather.23 = bf16[352,1024]{0,1:T(8,128)(2,1)} all-gather(bf16[352,32]{0,1:T(8,128)(2,1)S(1)} %copy-done.15), channel_id=1, replica_groups=mesh['rep'=2,'fs'=32,'tp_0'=4,'tp_1'=2] {'fs'}, dimensions={1}, use_global_device_ids=true | all-gather | bytes 743424 | tf_op jit(solution)/shard_map/all_gather | solution.py:241
  490.3 84.7 %all-gather.7.cloned.1.call-done = bf16[720896]{0:T(1024)(128)(2,1)} async-done(((bf16[22528]{0:T(1024)(128)(2,1)}), bf16[720896]{0:T(1024)(128)(2,1)}) %all-gather.7.cloned.1.call-update) | async-done | bytes 1441808 | tf_op jit(solution)/shard_map/all_gather | solution.py:23
  575.0 1.7 reshape.444
  577.5 4.1 all-to-all-start.6
  581.7 1.6 all-to-all-done.6
  583.3 4.6 all_to_all.41
  587.8 2.1 stack.31
  589.9 4.4 all-to-all-start.7
  594.3 1.2 fusion.100
  595.5 3.1 reshape_reshape.26
  598.7 2.1 reshape_reshape.25
  600.8 8.9 %all-to-all-done.7 = bf16[4,2,64,1024]{3,2,1,0:T(8,128)(2,1)S(1)} async-done(((bf16[4,2,64,1024]{3,2,1,0:T(8,128)(2,1)}), bf16[4,2,64,1024]{3,2,1,0:T(8,128)(2,1)S(1)}, u32[]{:S(2)}, u32[]{:S(2)}) %all-to-all-start.7) | async-done | bytes 1048608 | tf_op jit(solution)/shard_map/all_to_all | solution.py:40
  610.8 1.0 fusion.19
  612.0 1.0 fusion.20
  613.1 4.7 convolution_convert_fusion
  617.9 47.4 %reduce-scatter.5.cloned.1.call-done = bf16[128,1024]{1,0:T(8,128)(2,1)} async-done(((bf16[1024,1024]{1,0:T(8,128)(2,1)}), bf16[128,1024]{1,0:T(8,128)(2,1)}) %reduce-scatter.5.cloned.1.call-update) | async-done | bytes 262160 | tf_op jit(solution)/shard_map/reduce_scatter | solution.py:67
  665.3 1.1 fusion.38
  666.4 1.8 fusion.74
  (142 shorter events, 39.1 us)
Async XLA Ops:
  6.5 220.8 %all-gather.5.cloned.1.call-start = ((), (), s32[]{:S(2)}) async-start(), calls=%async_computation.12 | async-start | bytes 1622016 | tf_op jit(solution)/shard_map/all_gather | solution.py:23
  10.4 6.3 copy-start.24
  12.4 13.8 %all-to-all-start = ((bf16[4,1,64,1024]{3,2,1,0:T(8,128)(2,1)}), bf16[4,1,64,1024]{3,2,1,0:T(8,128)(2,1)S(1)}, u32[]{:S(2)}, u32[]{:S(2)}) async-start(bf16[4,1,64,1024]{3,2,1,0:T(8,128)(2,1)} %stack.24), calls=%async_computation | async-start | bytes 1048576 | tf_op jit(solution)/shard_map/all_to_all | solution.py:40
  26.2 5.0 all-to-all-start.2
  36.9 4.9 copy-start.18
  36.9 129.3 %all-to-all-start.3 = ((bf16[4,2,64,1024]{3,2,1,0:T(8,128)(2,1)}), bf16[4,2,64,1024]{3,2,1,0:T(8,128)(2,1)S(1)}, u32[]{:S(2)}, u32[]{:S(2)}) async-start(bf16[4,2,64,1024]{3,2,1,0:T(8,128)(2,1)} %stack.27), calls=%async_computation.3 | async-start | bytes 2097152 | tf_op jit(solution)/shard_map/all_to_all | solution.py:40
  40.5 320.5 %reduce-scatter.3.cloned.1.call-start = ((), (), s32[]{:S(2)}) async-start(), calls=%async_computation.10 | async-start | bytes 2359296 | tf_op jit(solution)/shard_map/reduce_scatter | solution.py:67
  235.9 0.8 copy-start.28
  245.5 3.0 copy-start.3
  245.5 3.0 copy-start.4
  251.4 16.6 %copy-start.11 = (bf16[1024,128]{0,1:T(8,128)(2,1)S(1)}, bf16[1024,128]{0,1:T(8,128)(2,1)}, u32[]{:S(2)}) copy-start(bf16[1024,128]{0,1:T(8,128)(2,1)} %get-tuple-element.170) | copy-start | bytes 786436
  272.0 1.8 copy-start.6
  272.0 1.8 copy-start.27
  275.6 14.1 %copy-start.1 = (f32[8,256,128]{1,2,0:T(8,128)S(1)}, f32[8,256,128]{1,2,0:T(8,128)}, u32[]{:S(2)}) copy-start(f32[8,256,128]{1,2,0:T(8,128)} %fusion.105) | copy-start | bytes 3145732
  293.0 9.0 %copy-start = (f32[8,256,128]{1,2,0:T(8,128)S(1)}, f32[8,256,128]{1,2,0:T(8,128)}, u32[]{:S(2)}) copy-start(f32[8,256,128]{1,2,0:T(8,128)} %fusion.104) | copy-start | bytes 3145732
  293.0 9.0 %copy-start.8 = (bf16[1024,1,128]{2,0,1:T(8,128)(2,1)S(1)}, bf16[1024,1,128]{2,0,1:T(8,128)(2,1)}, u32[]{:S(2)}) copy-start(bf16[1024,1,128]{2,0,1:T(8,128)(2,1)} %copy.43) | copy-start | bytes 786436
  302.0 2.5 copy-start.2
  311.9 0.7 copy-start.16
  311.9 0.8 copy-start.17
  311.9 1.6 copy-start.22
  311.9 1.6 copy-start.23
  311.9 50.2 %copy-start.7 = (bf16[1,128,1024]{2,1,0:T(8,128)(2,1)S(1)}, bf16[1,128,1024]{2,1,0:T(8,128)(2,1)}, u32[]{:S(2)}) copy-start(bf16[1,128,1024]{2,1,0:T(8,128)(2,1)} %param.22) | copy-start | bytes 786436
  312.0 50.2 %copy-start.19 = (f32[1024]{0:T(1024)S(1)}, f32[1024]{0:T(1024)}, u32[]{:S(2)}) copy-start(f32[1024]{0:T(1024)} %param.30) | copy-start | bytes 12292
  312.0 52.1 %copy-start.20 = (f32[1024]{0:T(1024)S(1)}, f32[1024]{0:T(1024)}, u32[]{:S(2)}) copy-start(f32[1024]{0:T(1024)} %param.31) | copy-start | bytes 12292
  312.0 263.0 %all-gather.7.cloned.1.call-start = ((), (), s32[]{:S(2)}) async-start(), calls=%async_computation.13 | async-start | bytes 1486848 | tf_op jit(solution)/shard_map/all_gather | solution.py:23
  363.4 0.7 copy-start.9
  363.4 5.2 copy-start.15
  365.1 212.4 %all-to-all-start.4 = ((bf16[4,1,64,1024]{3,2,1,0:T(8,128)(2,1)}), bf16[4,1,64,1024]{3,2,1,0:T(8,128)(2,1)S(1)}, u32[]{:S(2)}, u32[]{:S(2)}) async-start(bf16[4,1,64,1024]{3,2,1,0:T(8,128)(2,1)} %stack.28), calls=%async_computation.5 | async-start | bytes 1048576 | tf_op jit(solution)/shard_map/all_to_all | solution.py:40
  577.5 5.8 all-to-all-start.6
  589.9 19.8 %all-to-all-start.7 = ((bf16[4,2,64,1024]{3,2,1,0:T(8,128)(2,1)}), bf16[4,2,64,1024]{3,2,1,0:T(8,128)(2,1)S(1)}, u32[]{:S(2)}, u32[]{:S(2)}) async-start(bf16[4,2,64,1024]{3,2,1,0:T(8,128)(2,1)} %stack.31), calls=%async_computation.8 | async-start | bytes 2097152 | tf_op jit(solution)/shard_map/all_to_all | solution.py:40
  594.3 71.0 %reduce-scatter.5.cloned.1.call-start = ((), (), s32[]{:S(2)}) async-start(), calls=%async_computation.11 | async-start | bytes 2359296 | tf_op jit(solution)/shard_map/reduce_scatter | solution.py:67
  595.5 3.1 copy-start.5
  609.7 1.1 copy-start.13
  610.8 1.1 copy-start.14
  612.0 1.1 copy-start.12
  612.0 1.1 copy-start.25
  612.0 1.1 copy-start.26
  612.0 1.1 copy-start.29
  612.0 1.1 copy-start.30
  617.9 48.5 %copy-start.10 = (bf16[128,1024]{1,0:T(8,128)(2,1)S(1)}, bf16[128,1024]{1,0:T(8,128)(2,1)}, u32[]{:S(2)}) copy-start(bf16[128,1024]{1,0:T(8,128)(2,1)} %copy-done.9) | copy-start | bytes 786436
  617.9 48.5 %copy-start.21 = (f32[1024]{0:T(1024)S(1)}, f32[1024]{0:T(1024)}, u32[]{:S(2)}) copy-start(f32[1024]{0:T(1024)} %param.39) | copy-start | bytes 12292
Sparse Core Ops, SparseCore 0:
  9.5 217.8 all-gather.4
  312.1 48.8 reduce-scatter.2
  363.1 211.8 all-gather.6
  618.0 47.2 reduce-scatter.4
